TPU v7x, 32 devices: a whole 2x2x4 slice. The times are simulated.
32 devices in a mesh: grp: 2 (over x), kv: 4 (over y, core), tp: 4 (over z).
Axes of the slice: x: 2, y: 2, z: 4, core: 2. Of those that a mesh axis runs over, the one named last changes fastest.
Arguments:
- tokens: bfloat16 [64, 4096], P('grp', ('kv', 'tp')), parts along dimension 0, may hold values from -12 to 12
- gain_in: bfloat16 [4096], P(('kv', 'tp')), may hold values from 0.099609375 to 1.8984375
- gate_in: bfloat16 [4096, 11008], P('kv', 'tp'), may hold values from -0.09375 to 0.09375
- up_in: bfloat16 [4096, 11008], P('kv', 'tp'), may hold values from -0.09375 to 0.09375
- down_in: bfloat16 [11008, 4096], P('tp', 'kv'), may hold values from -0.21875 to 0.21875
- gain_mix: bfloat16 [4096], P(('kv', 'tp')), may hold values from 0.099609375 to 1.8984375
- w_query: bfloat16 [4096, 1024], P('kv', 'tp'), may hold values from -0.09375 to 0.09375
- w_key: bfloat16 [4096, 1024], P('kv', 'tp'), may hold values from -0.09375 to 0.09375
- w_value: bfloat16 [4096, 2048], P('kv', 'tp'), may hold values from -0.09375 to 0.09375
- w_gate: bfloat16 [4096, 2048], P('kv', 'tp'), may hold values from -0.09375 to 0.09375
- w_mixout: bfloat16 [2048, 4096], P('tp', 'kv'), may hold values from -0.125 to 0.125
- forget_rate: float32 [8], P('tp'), may hold values from 0.01 to 0.7
- state_in: float32 [64, 8, 128, 256], P(('grp', 'kv'), 'tp'), parts along dimension 0, may hold values from -0.6 to 0.6
- positions: int32 [64], P(('grp', 'kv')), parts along dimension 0, may hold values from 0 to 8191
- gain_out: bfloat16 [4096], P(('kv', 'tp')), may hold values from 0.099609375 to 1.8984375
- gate_out: bfloat16 [4096, 11008], P('kv', 'tp'), may hold values from -0.09375 to 0.09375
- up_out: bfloat16 [4096, 11008], P('kv', 'tp'), may hold values from -0.09375 to 0.09375
- down_out: bfloat16 [11008, 4096], P('tp', 'kv'), may hold values from -0.21875 to 0.21875
Outputs:
- result: bfloat16 [64, 4096], P('grp', ('kv', 'tp')), parts along dimension 0
- new_state: float32 [64, 8, 128, 256], P(('grp', 'kv'), 'tp'), parts along dimension 0
There are 2 independent parts, one for each index of `grp`. A program takes and returns all parts, laid end to end along the dimension named above; an argument that names none is the same for every part. Nothing has to cross between parts.
All inputs are finite; a program needn't handle non-finite values.
Results may differ from a plain program's by a relative error of at most 0.024.
Values may be sent and summed in bfloat16 or wider, within the bound.
A program may use at most 128 MiB of HBM per device.

v0:
```python
import jax
import jax.numpy as jnp
from jax import lax
from jax.sharding import PartitionSpec as P

D = 4096
DK = 128
DV = 256


epsilon = 1e-06


def rotate(vectors, positions):
    half_dim = vectors.shape[-1] // 2
    inverse = jnp.power(10000.0, -jnp.arange(half_dim, dtype=jnp.float32) * 2.0 / vectors.shape[-1])
    angles = positions.astype(jnp.float32)[:, None] * inverse[None, :]
    cosine = jnp.cos(angles)[:, None, :]
    sine_part = jnp.sin(angles)[:, None, :]
    first_half = vectors[..., :half_dim]
    second_half = vectors[..., half_dim:]
    return jnp.concatenate(
        [
            first_half * cosine - second_half * sine_part,
            first_half * sine_part + second_half * cosine,
        ],
        axis=-1,
    )


def block_rows(tokens, gain_row):
    raw_block, gain_block = (
        lax.all_gather(tokens, "tp", axis=1, tiled=True),
        lax.all_gather(gain_row[None, :], "tp", axis=1, tiled=True),
    )
    wide_block = raw_block.astype(jnp.float32)
    squares = lax.psum(jnp.sum(wide_block * wide_block, axis=1), "kv")
    normed = (wide_block * gain_block.astype(jnp.float32)).astype(jnp.bfloat16)
    return (normed, lax.rsqrt(squares / D + epsilon))


def half_mlp(tokens, gain_row, w_gate, w_up, w_down):
    widened = tokens.astype(jnp.float32)
    normed, factor = block_rows(tokens, gain_row)
    gate_part = jnp.dot(normed, w_gate, preferred_element_type=jnp.float32)
    up_part = jnp.dot(normed, w_up, preferred_element_type=jnp.float32)
    gate_sum, up_sum = (
        lax.psum(gate_part.astype(jnp.bfloat16), "kv").astype(jnp.float32),
        lax.psum(up_part.astype(jnp.bfloat16), "kv").astype(jnp.float32),
    )
    column = factor[:, None]
    hidden = (jax.nn.silu(column * gate_sum) * (column * up_sum)).astype(jnp.bfloat16)
    partial_value = jnp.dot(hidden, w_down, preferred_element_type=jnp.float32)
    lowered = lax.psum_scatter(
        partial_value.astype(jnp.bfloat16), "tp", scatter_dimension=1, tiled=True
    ).astype(jnp.float32)
    return (widened + 0.5 * lowered).astype(jnp.bfloat16)


def on_device(
    tokens,
    gain_in,
    gate_in,
    up_in,
    down_in,
    gain_mix,
    w_query,
    w_key,
    w_value,
    w_gate,
    w_mixout,
    forget_rate,
    state_in,
    positions,
    gain_out,
    gate_out,
    up_out,
    down_out,
):
    after_first = half_mlp(tokens, gain_in, gate_in, up_in, down_in)
    widened = after_first.astype(jnp.float32)
    own_rows = state_in.shape[0]
    normed, factor_all = block_rows(after_first, gain_mix)
    head_count = w_query.shape[1] // DK
    weights = (w_query, w_key, w_value, w_gate)
    projected = lax.psum_scatter(
        jnp.concatenate(
            [jnp.dot(normed, weight, preferred_element_type=jnp.float32) for weight in weights],
            axis=1,
        ).astype(jnp.bfloat16),
        "kv",
        scatter_dimension=0,
        tiled=True,
    ).astype(jnp.float32)
    factor = lax.dynamic_slice_in_dim(factor_all, lax.axis_index("kv") * own_rows, own_rows)[
        :, None
    ]
    rounded = lax.optimization_barrier((factor * projected).astype(jnp.bfloat16))
    scaled = rounded.astype(jnp.float32)
    bounds = [head_count * DK, 2 * head_count * DK, 2 * head_count * DK + head_count * DV]
    sections = jnp.split(scaled, bounds, axis=1)
    queries = rotate(sections[0].reshape(own_rows, head_count, DK), positions)
    key_rot = rotate(sections[1].reshape(own_rows, head_count, DK), positions) * DK ** (-0.5)
    values_now = sections[2].reshape(own_rows, head_count, DV)
    gates_now = sections[3].reshape(own_rows, head_count, DV)
    decays = jnp.exp(-forget_rate)
    carried = jnp.einsum("bhd,bhde->bhe", queries, state_in, precision=lax.Precision.HIGHEST)
    present = jnp.sum(queries * key_rot, axis=-1, keepdims=True) * values_now
    retained = present + decays[None, :, None] * carried
    new_state = (
        decays[None, :, None, None] * state_in + key_rot[..., None] * values_now[..., None, :]
    )
    normed_heads = retained * lax.rsqrt(
        jnp.mean(retained * retained, axis=-1, keepdims=True) + epsilon
    )
    mixed = (
        (jax.nn.silu(gates_now) * normed_heads)
        .astype(jnp.bfloat16)
        .reshape(own_rows, head_count * DV)
    )
    head_terms = jnp.dot(
        lax.all_gather(mixed, "kv", axis=0, tiled=True),
        w_mixout,
        preferred_element_type=jnp.float32,
    )
    mixed_sum = lax.psum_scatter(
        head_terms.astype(jnp.bfloat16), "tp", scatter_dimension=1, tiled=True
    ).astype(jnp.float32)
    second = (widened + mixed_sum).astype(jnp.bfloat16)
    result = half_mlp(second, gain_out, gate_out, up_out, down_out)
    return (result, new_state)


def solution(mesh):
    in_specs = (
        P("grp", ("kv", "tp")),
        P(("kv", "tp")),
        P("kv", "tp"),
        P("kv", "tp"),
        P("tp", "kv"),
        P(("kv", "tp")),
        P("kv", "tp"),
        P("kv", "tp"),
        P("kv", "tp"),
        P("kv", "tp"),
        P("tp", "kv"),
        P("tp"),
        P(("grp", "kv"), "tp", None, None),
        P(("grp", "kv")),
        P(("kv", "tp")),
        P("kv", "tp"),
        P("kv", "tp"),
        P("tp", "kv"),
    )
    out_specs = (P("grp", ("kv", "tp")), P(("grp", "kv"), "tp", None, None))
    return jax.shard_map(
        on_device, mesh=mesh, in_specs=in_specs, out_specs=out_specs, check_vma=False
    )
```

profile of v0, /device:TPU:0, one launch (start us, length us, event | category | flops | bytes accessed | tf_op | source)
XLA Modules:
  0.0 262.1 jit_solution(9441796536752481727)
XLA Ops:
  8.0 12.8 %all-gather.3 = bf16[4,1,256]{2,1,0:T(2,128)(2,1)S(1)} all-gather(bf16[1,1,256]{2,1,0:T(2,128)(2,1)S(1)} %reshape.117), channel_id=2, replica_groups=mesh['grp'=2,'kv'=4,'tp'=4] {'tp'}, dimensions={0}, use_global_device_ids=true | all-gather | bytes 2560 | tf_op jit(solution)/shard_map/all_gather | solution.py:34
  20.8 13.3 %all_gather.21 = bf16[32,1024]{1,0:T(8,128)(2,1)S(1)} all-gather(bf16[32,256]{1,0:T(8,128)(2,1)} %param.18), channel_id=1, replica_groups=mesh['grp'=2,'kv'=4,'tp'=4] {'tp'}, dimensions={1}, use_global_device_ids=true | all-gather | bytes 81920 | tf_op jit(solution)/shard_map/all_gather | solution.py:33
  34.2 5.1 %convolution_convert_fusion.2 = bf16[32,2752]{1,0:T(8,128)(2,1)} fusion(bf16[1024,2752]{0,1:T(8,128)(2,1)} %param.21, bf16[32,1024]{1,0:T(8,128)(2,1)S(1)} %all_gather.21, f32[1024]{0:T(1024)S(1)} %bitcast.43), kind=kOutput, calls=%fused_computation.2 | convolution fusion | flops 180541440 | bytes 5881856 | tf_op jit(solution)/shard_map/dot_general | solution.py:46
  39.2 2.4 convolution_convert_fusion.3
  41.9 7.8 %all-gather.4 = bf16[4,1,256]{2,1,0:T(2,128)(2,1)S(1)} all-gather(bf16[1,1,256]{2,1,0:T(2,128)(2,1)S(1)} %reshape.119), channel_id=3, replica_groups=mesh['grp'=2,'kv'=4,'tp'=4] {'tp'}, dimensions={0}, use_global_device_ids=true | all-gather | bytes 2560 | tf_op jit(solution)/shard_map/all_gather | solution.py:34
  49.7 6.1 %psum.49 = f32[32]{0:T(128)S(1)} all-reduce(f32[32]{0:T(128)S(1)} %fusion.4), channel_id=1, replica_groups=mesh['grp'=2,'kv'=4,'tp'=4] {'kv'}, use_global_device_ids=true, to_apply=%region_1.0 | all-reduce | flops 32 | bytes 256 | tf_op jit(solution)/shard_map/psum | solution.py:37
  55.9 16.9 %all-reduce.7.cloned.1.call-done = (bf16[32,2752]{1,0:T(8,128)(2,1)}, bf16[32,2752]{1,0:T(8,128)(2,1)}) async-done(((bf16[32,2752]{1,0:T(8,128)(2,1)}, bf16[32,2752]{1,0:T(8,128)(2,1)}), (bf16[32,2752]{1,0:T(8,128)(2,1)}, bf16[32,2752]{1,0:T(8,128)(2,1)})) %all-reduce.7.cloned.1.call-update) | async-done | bytes 352272 | tf_op jit(solution)/shard_map/psum | solution.py:49
  72.9 4.6 %convolution_convert_fusion.6 = bf16[32,1024]{1,0:T(8,128)(2,1)} fusion(bf16[2752,1024]{1,0:T(8,128)(2,1)} %param.22, bf16[32,2752]{1,0:T(8,128)(2,1)} %get-tuple-element.4, bf16[32,2752]{1,0:T(8,128)(2,1)} %get-tuple-element.5, f32[32]{0:T(128)S(1)} %add_rsqrt_fusion.3), kind=kOutput, calls=%fused_computation.7 | convolution fusion | flops 181268480 | bytes 6054016 | tf_op jit(solution)/shard_map/dot_general | solution.py:53
  77.5 19.4 %reduce-scatter.5.cloned.1.call-done = bf16[32,256]{1,0:T(8,128)(2,1)} async-done(((bf16[32,1024]{1,0:T(8,128)(2,1)}), bf16[32,256]{1,0:T(8,128)(2,1)}) %reduce-scatter.5.cloned.1.call-update) | async-done | bytes 16400 | tf_op jit(solution)/shard_map/reduce_scatter | solution.py:54
  97.7 13.1 %all_gather.23 = bf16[32,1024]{1,0:T(8,128)(2,1)S(1)} all-gather(bf16[32,256]{1,0:T(8,128)(2,1)S(1)} %add_convert_fusion.2), channel_id=1, replica_groups=mesh['grp'=2,'kv'=4,'tp'=4] {'tp'}, dimensions={1}, use_global_device_ids=true | all-gather | bytes 81920 | tf_op jit(solution)/shard_map/all_gather | solution.py:33
  110.9 5.7 %psum.52 = f32[32]{0:T(128)S(1)} all-reduce(f32[32]{0:T(128)S(1)} %fusion.6), channel_id=1, replica_groups=mesh['grp'=2,'kv'=4,'tp'=4] {'kv'}, use_global_device_ids=true, to_apply=%region_6.7 | all-reduce | flops 32 | bytes 256 | tf_op jit(solution)/shard_map/psum | solution.py:37
  120.5 1.5 convolution_convert_fusion.7
  122.9 18.0 %reduce-scatter.7.cloned.1.call-done = bf16[8,1536]{1,0:T(8,128)(2,1)} async-done(((bf16[32,1536]{1,0:T(8,128)(2,1)}), bf16[8,1536]{1,0:T(8,128)(2,1)}) %reduce-scatter.7.cloned.1.call-update) | async-done | bytes 24592 | tf_op jit(solution)/shard_map/reduce_scatter | solution.py:86
  143.3 5.2 %all_gather.25 = bf16[32,512]{1,0:T(8,128)(2,1)S(1)} all-gather(bf16[8,512]{1,0:T(8,128)(2,1)S(1)} %bitcast.45), channel_id=1, replica_groups=mesh['grp'=2,'kv'=4,'tp'=4] {'kv'}, dimensions={0}, use_global_device_ids=true | all-gather | bytes 40960 | tf_op jit(solution)/shard_map/all_gather | solution.py:122
  149.5 10.9 %all-gather.5 = bf16[4,1,256]{2,1,0:T(2,128)(2,1)S(1)} all-gather(bf16[1,1,256]{2,1,0:T(2,128)(2,1)S(1)} %reshape.121), channel_id=4, replica_groups=mesh['grp'=2,'kv'=4,'tp'=4] {'tp'}, dimensions={0}, use_global_device_ids=true | all-gather | bytes 2560 | tf_op jit(solution)/shard_map/all_gather | solution.py:34
  160.5 8.4 %reduce-scatter.9.cloned.1.call-done = bf16[32,256]{1,0:T(8,128)(2,1)} async-done(((bf16[32,1024]{1,0:T(8,128)(2,1)}), bf16[32,256]{1,0:T(8,128)(2,1)}) %reduce-scatter.9.cloned.1.call-update) | async-done | bytes 16400 | tf_op jit(solution)/shard_map/reduce_scatter | solution.py:126
  169.6 13.1 %all_gather.26 = bf16[32,1024]{1,0:T(8,128)(2,1)S(1)} all-gather(bf16[32,256]{1,0:T(8,128)(2,1)S(1)} %add_convert_fusion.1), channel_id=1, replica_groups=mesh['grp'=2,'kv'=4,'tp'=4] {'tp'}, dimensions={1}, use_global_device_ids=true | all-gather | bytes 81920 | tf_op jit(solution)/shard_map/all_gather | solution.py:33
  182.8 5.7 %psum.53 = f32[32]{0:T(128)S(1)} all-reduce(f32[32]{0:T(128)S(1)} %fusion.8), channel_id=1, replica_groups=mesh['grp'=2,'kv'=4,'tp'=4] {'kv'}, use_global_device_ids=true, to_apply=%region_12.13 | all-reduce | flops 32 | bytes 256 | tf_op jit(solution)/shard_map/psum | solution.py:37
  188.5 5.0 %convolution_convert_fusion = bf16[32,2752]{1,0:T(8,128)(2,1)} fusion(bf16[1024,2752]{0,1:T(8,128)(2,1)} %param.34, bf16[32,1024]{1,0:T(8,128)(2,1)S(1)} %all_gather.26, f32[1024]{0:T(1024)S(1)} %bitcast.41), kind=kOutput, calls=%fused_computation | convolution fusion | flops 180541440 | bytes 5881856 | tf_op jit(solution)/shard_map/dot_general | solution.py:46
  193.5 5.0 %convolution_convert_fusion.1 = bf16[32,2752]{1,0:T(8,128)(2,1)} fusion(bf16[1024,2752]{0,1:T(8,128)(2,1)} %param.33, bf16[32,1024]{1,0:T(8,128)(2,1)S(1)} %all_gather.26, f32[1024]{0:T(1024)S(1)} %bitcast.42), kind=kOutput, calls=%fused_computation.1 | convolution fusion | flops 180541440 | bytes 5881856 | tf_op jit(solution)/shard_map/dot_general | solution.py:45
  198.6 31.3 %all-reduce.5.cloned.1.call-done = (bf16[32,2752]{1,0:T(8,128)(2,1)}, bf16[32,2752]{1,0:T(8,128)(2,1)}) async-done(((bf16[32,2752]{1,0:T(8,128)(2,1)}, bf16[32,2752]{1,0:T(8,128)(2,1)}), (bf16[32,2752]{1,0:T(8,128)(2,1)}, bf16[32,2752]{1,0:T(8,128)(2,1)})) %all-reduce.5.cloned.1.call-update) | async-done | bytes 352272 | tf_op jit(solution)/shard_map/psum | solution.py:49
  229.9 4.6 %convolution_convert_fusion.4 = bf16[32,1024]{1,0:T(8,128)(2,1)} fusion(bf16[2752,1024]{1,0:T(8,128)(2,1)} %param.35, bf16[32,2752]{1,0:T(8,128)(2,1)} %get-tuple-element.2, bf16[32,2752]{1,0:T(8,128)(2,1)} %get-tuple-element.3, f32[32]{0:T(128)S(1)} %add_rsqrt_fusion.1), kind=kOutput, calls=%fused_computation.5 | convolution fusion | flops 181268480 | bytes 6054016 | tf_op jit(solution)/shard_map/dot_general | solution.py:53
  234.5 1.7 multiply_add_fusion
  236.2 17.8 %reduce-scatter.11.cloned.1.call-done = bf16[32,256]{1,0:T(8,128)(2,1)} async-done(((bf16[32,1024]{1,0:T(8,128)(2,1)}), bf16[32,256]{1,0:T(8,128)(2,1)}) %reduce-scatter.11.cloned.1.call-update) | async-done | bytes 16400 | tf_op jit(solution)/shard_map/reduce_scatter | solution.py:54
  (65 shorter events, 12.6 us)
Async XLA Ops:
  7.2 141.4 %copy-start = (bf16[512,1024]{1,0:T(8,128)(2,1)S(1)}, bf16[512,1024]{1,0:T(8,128)(2,1)}, u32[]{:S(2)}) copy-start(bf16[512,1024]{1,0:T(8,128)(2,1)} %param.28) | copy-start | bytes 3145732
  7.2 65.7 %all-reduce.7.cloned.1.call-start = ((), (), s32[]{:S(2)}) async-start(), calls=%async_computation.9 | async-start | bytes 720896 | tf_op jit(solution)/shard_map/psum | solution.py:49
  7.2 32.0 %copy-start.2 = (bf16[1024,2752]{0,1:T(8,128)(2,1)S(1)}, bf16[1024,2752]{0,1:T(8,128)(2,1)}, u32[]{:S(2)}) copy-start(bf16[1024,2752]{0,1:T(8,128)(2,1)} %param.20) | copy-start | bytes 16908292
  34.2 7.7 %copy-start.4 = (s32[8]{0:T(128)S(1)}, s32[8]{0:T(128)}, u32[]{:S(2)}) copy-start(s32[8]{0:T(128)} %param.31) | copy-start | bytes 100
  34.2 7.7 %copy-start.5 = (bf16[256]{0:T(256)(128)(2,1)S(1)}, bf16[256]{0:T(256)(128)(2,1)}, u32[]{:S(2)}) copy-start(bf16[256]{0:T(256)(128)(2,1)} %param.23) | copy-start | bytes 1540
  39.2 38.3 %copy-start.6 = (f32[2]{0:T(128)S(1)}, f32[2]{0:T(128)}, u32[]{:S(2)}) copy-start(f32[2]{0:T(128)} %param.29) | copy-start | bytes 28
  39.2 57.7 %copy-start.3 = (bf16[32,256]{1,0:T(8,128)(2,1)S(1)}, bf16[32,256]{1,0:T(8,128)(2,1)}, u32[]{:S(2)}) copy-start(bf16[32,256]{1,0:T(8,128)(2,1)} %param.18) | copy-start | bytes 49156
  41.7 100.3 %copy-start.1 = (f32[8,2,128,256]{3,2,1,0:T(8,128)S(1)}, f32[8,2,128,256]{3,2,1,0:T(8,128)}, u32[]{:S(2)}) copy-start(f32[8,2,128,256]{3,2,1,0:T(8,128)} %param.30) | copy-start | bytes 6291460
  41.7 55.2 %reduce-scatter.5.cloned.1.call-start = ((), (), s32[]{:S(2)}) async-start(), calls=%async_computation.4 | async-start | bytes 81920 | tf_op jit(solution)/shard_map/reduce_scatter | solution.py:54
  72.9 76.7 %copy-start.7 = (bf16[256]{0:T(256)(128)(2,1)S(1)}, bf16[256]{0:T(256)(128)(2,1)}, u32[]{:S(2)}) copy-start(bf16[256]{0:T(256)(128)(2,1)} %param.32) | copy-start | bytes 1540
  77.5 63.4 %reduce-scatter.7.cloned.1.call-start = ((), (), s32[]{:S(2)}) async-start(), calls=%async_computation.5 | async-start | bytes 122880 | tf_op jit(solution)/shard_map/reduce_scatter | solution.py:86
  122.7 46.1 %reduce-scatter.9.cloned.1.call-start = ((), (), s32[]{:S(2)}) async-start(), calls=%async_computation.6 | async-start | bytes 81920 | tf_op jit(solution)/shard_map/reduce_scatter | solution.py:126
  149.5 80.4 %all-reduce.5.cloned.1.call-start = ((), (), s32[]{:S(2)}) async-start(), calls=%async_computation.8 | async-start | bytes 720896 | tf_op jit(solution)/shard_map/psum | solution.py:49
  198.6 55.4 %reduce-scatter.11.cloned.1.call-start = ((), (), s32[]{:S(2)}) async-start(), calls=%async_computation.7 | async-start | bytes 81920 | tf_op jit(solution)/shard_map/reduce_scatter | solution.py:54
Sparse Core Ops, SparseCore 0:
  41.8 31.0 all-reduce.6
  77.6 19.2 reduce-scatter.4
  122.8 18.0 reduce-scatter.6
  149.6 19.2 reduce-scatter.8
  198.7 31.1 all-reduce.4
  234.6 19.2 reduce-scatter.10
where the time goes:
time: 263 us; the launch traced here: 262 us
  waiting for transfers between devices  112 us (43%)
  blocking collectives  93.6 us (36%)
  matrix products  34.2 us (13%)
  between operations  14.3 us (5%)
  other arithmetic  6.92 us (3%)
    psum x2, waiting for transfers between devices, half_mlp(): lax.psum(up_part.astype(jnp.bfloat16), 'kv').astype(jnp.float32)  48.2 us
    all_gather x3, blocking collectives, block_rows(): lax.all_gather(tokens, 'tp', axis=1, tiled=True)  39.6 us
    reduce_scatter x2, waiting for transfers between devices, half_mlp(): lax.psum_scatter(partial_value.astype(jnp.bfloat16), 'tp', scatter_dimens...  37.2 us
    all_gather x3, blocking collectives, block_rows(): lax.all_gather(gain_row[None, :], 'tp', axis=1, tiled=True)  31.4 us
    reduce_scatter x1, waiting for transfers between devices, on_device(): lax.psum_scatter(jnp.concatenate([jnp.dot(normed, weight, preferred_eleme...  18 us
    psum x3, blocking collectives, block_rows(): squares = lax.psum(jnp.sum(wide_block * wide_block, axis=1), 'kv')  17.4 us
    dot_general x2, matrix products, half_mlp(): up_part = jnp.dot(normed, w_up, preferred_element_type=jnp.float32)  10.1 us
    dot_general x2, matrix products, half_mlp(): partial_value = jnp.dot(hidden, w_down, preferred_element_type=jnp.float32)  9.16 us
  transfers between devices with their start and end apart: 6, of which 6 were waited for; matrix products, arithmetic and copies ran while one was open for 1% of the time, Pallas kernels for 0%

commit v1 on v0

--- a/solution.py
+++ b/solution.py
@@ -1,6 +1,11 @@
+import functools
+import math
+
 import jax
 import jax.numpy as jnp
 from jax import lax
+from jax.experimental import pallas as pl
+from jax.experimental.pallas import tpu as pltpu
 from jax.sharding import PartitionSpec as P
 
 D = 4096
@@ -131,6 +136,511 @@
     return (result, new_state)
 
 
+MESH = pl.DeviceIdType.MESH
+TILE = 256
+CHUNKS = 3
+
+
+def chunk_bounds(width):
+    tiles = max(1, width // TILE)
+    count = min(CHUNKS, tiles)
+    edges = [tiles * c // count * TILE for c in range(count)] + [width]
+    return list(zip(edges[:-1], edges[1:]))
+
+
+def times_transposed(lhs, rhs):
+    return lax.dot_general(
+        lhs, rhs, (((1,), (1,)), ((), ())), preferred_element_type=jnp.float32
+    )
+
+
+def ceil_lanes(width):
+    return -(-width // 128) * 128
+
+
+def silu(values):
+    return values / (1.0 + jnp.exp(-values))
+
+
+def sine_pair(angles):
+    turns = jnp.floor(angles * (0.5 / math.pi) + 0.5)
+    rest = angles - turns * 6.28125
+    rest = rest - turns * (2.0 * math.pi - 6.28125)
+    square = rest * rest
+    cosine = jnp.zeros_like(rest)
+    sine = jnp.zeros_like(rest)
+    for power in range(9, -1, -1):
+        cosine = cosine * square + (-1.0) ** power / math.factorial(2 * power)
+        sine = sine * square + (-1.0) ** power / math.factorial(2 * power + 1)
+    return cosine, sine * rest
+
+
+def layer_kernel(
+    n_kv,
+    n_tp,
+    tokens,
+    gain_in,
+    gain_mix,
+    gain_out,
+    forget,
+    positions,
+    gate_in,
+    up_in,
+    down_in,
+    w_query,
+    w_key,
+    w_value,
+    w_gate,
+    w_mixout,
+    state_in,
+    gate_out,
+    up_out,
+    down_out,
+    result,
+    new_state,
+    gate_v,
+    up_v,
+    down_v,
+    query_v,
+    key_v,
+    value_v,
+    gates_v,
+    mixout_v,
+    state_v,
+    gains_all,
+    feat_all,
+    sums_send,
+    sums_recv,
+    hidden_all,
+    down_acc,
+    proj_send,
+    proj_recv,
+    mixed_all,
+    part_send,
+    part_recv,
+    load_sem,
+    store_sem,
+    send_sem,
+    recv_sem,
+):
+    kv, tp = lax.axis_index("kv"), lax.axis_index("tp")
+    rows, fb = tokens.shape
+    own = rows // n_kv
+    blk = fb * n_tp
+    ff = gate_in.shape[0]
+    ffp = ceil_lanes(ff)
+    _, heads, dk, dv = state_in.shape
+    chunks = chunk_bounds(ff)
+    full = blk * n_kv
+
+    pairs = []
+    for first, last in chunks:
+        span = pl.ds(first, last - first)
+        pairs.append((gate_in.at[span], gate_v.at[0, span]))
+        pairs.append((up_in.at[span], up_v.at[0, span]))
+    pairs += [
+        (down_in, down_v.at[0]),
+        (w_query, query_v),
+        (w_key, key_v),
+        (w_value, value_v),
+        (w_gate, gates_v),
+        (state_in, state_v),
+        (w_mixout, mixout_v),
+        (gate_out, gate_v.at[1]),
+        (up_out, up_v.at[1]),
+        (down_out, down_v.at[1]),
+    ]
+    loads = [
+        pltpu.make_async_copy(source, target, load_sem.at[place])
+        for place, (source, target) in enumerate(pairs)
+    ]
+    for load in loads:
+        load.start()
+    first_loads, loads = loads[: 2 * len(chunks)], loads[2 * len(chunks) :]
+
+    barrier = pltpu.get_barrier_semaphore()
+    for d in range(1, n_kv):
+        pl.semaphore_signal(
+            barrier, inc=1, device_id={"kv": lax.rem(kv + d, n_kv)}, device_id_type=MESH
+        )
+    for d in range(1, n_tp):
+        pl.semaphore_signal(
+            barrier, inc=1, device_id={"tp": lax.rem(tp + d, n_tp)}, device_id_type=MESH
+        )
+
+    sent = []
+
+    def exchange(stage, axis, source, target, place=None):
+        n, me = (n_kv, kv) if axis == "kv" else (n_tp, tp)
+        started = []
+        for d in range(1, n):
+            peer = lax.rem(me + d, n)
+            copy = pltpu.make_async_remote_copy(
+                src_ref=source(peer),
+                dst_ref=target.at[me] if place is None else place(target),
+                send_sem=send_sem.at[stage, d],
+                recv_sem=recv_sem.at[stage, d],
+                device_id={axis: peer},
+                device_id_type=MESH,
+            )
+            copy.start()
+            started.append(copy)
+        sent.extend(started)
+        return started
+
+    def arrive(copies):
+        for copy in copies:
+            copy.wait_recv()
+
+    def gathered_sum(send, recv, lanes):
+        total = send[kv, :, lanes].astype(jnp.float32)
+        for d in range(1, n_kv):
+            total += recv[lax.rem(kv + n_kv - d, n_kv), :, lanes].astype(jnp.float32)
+        return total
+
+    def put_rows(send, lanes, product):
+        for r in range(n_kv):
+            send[r, :, lanes] = product[r * own : (r + 1) * own].astype(jnp.bfloat16)
+
+    def put_squares(send, at, feats):
+        squares = jnp.sum(feats * feats, axis=1, keepdims=True)
+        high = squares.astype(jnp.bfloat16)
+        low = squares - high.astype(jnp.float32)
+        put_rows(send, pl.ds(at, 128), jnp.broadcast_to(high.astype(jnp.float32), (rows, 128)))
+        put_rows(send, pl.ds(at + 128, 128), jnp.broadcast_to(low, (rows, 128)))
+
+    def row_factor(send, recv, at):
+        high = gathered_sum(send, recv, pl.ds(at, 128))
+        low = gathered_sum(send, recv, pl.ds(at + 128, 128))
+        return lax.rsqrt((high + low)[:, :1] / full + epsilon)
+
+    def block(which, gain_at):
+        feats = jnp.concatenate(
+            [feat_all[which, t].astype(jnp.float32) for t in range(n_tp)], axis=1
+        )
+        gains = jnp.concatenate([gains_all[t, gain_at : gain_at + 1] for t in range(n_tp)], axis=1)
+        return feats, (feats * gains).astype(jnp.bfloat16)
+
+    def down_exchange(stage, which, lhs, weight, halve, residual, base=None):
+        copies = []
+        for d in list(range(1, n_tp)) + [0]:
+            t = lax.rem(tp + d, n_tp)
+            lanes = pl.ds(pl.multiple_of(t * fb, 128), fb)
+            product = jnp.dot(lhs, weight[:, lanes], preferred_element_type=jnp.float32)
+            if base is not None:
+                product += base[t]
+            part_send[which, t] = product.astype(jnp.bfloat16)
+            if d:
+                copy = pltpu.make_async_remote_copy(
+                    src_ref=part_send.at[which, t],
+                    dst_ref=part_recv.at[which, tp],
+                    send_sem=send_sem.at[stage, d],
+                    recv_sem=recv_sem.at[stage, d],
+                    device_id={"tp": t},
+                    device_id_type=MESH,
+                )
+                copy.start()
+                copies.append(copy)
+        sent.extend(copies)
+        total = part_send[which, tp].astype(jnp.float32)
+        for d, copy in enumerate(copies, 1):
+            copy.wait_recv()
+            total += part_recv[which, lax.rem(tp + n_tp - d, n_tp)].astype(jnp.float32)
+        return (residual.astype(jnp.float32) + halve * total).astype(jnp.bfloat16)
+
+    def half_block(which, stage, gain_at, weight_waits, down_wait, residual):
+        feats, normed = block(2 * which, gain_at)
+        send, recv = sums_send.at[which], sums_recv.at[which]
+        put_squares(send, 0, feats)
+        count = len(chunks)
+        going = []
+        for c, (first, last) in enumerate(chunks):
+            for wait in weight_waits[c]:
+                wait.wait()
+            padded = ceil_lanes(last - first)
+            gate_at = 256 + 2 * first
+            up_at = gate_at + padded
+
+            def step(column, width, first=first, gate_at=gate_at, up_at=up_at):
+                lines = pl.ds(first + column, width)
+                put_rows(
+                    send,
+                    pl.ds(gate_at + column, width),
+                    times_transposed(normed, gate_v[which, lines, :]),
+                )
+                put_rows(
+                    send,
+                    pl.ds(up_at + column, width),
+                    times_transposed(normed, up_v[which, lines, :]),
+                )
+
+            whole = (last - first) // TILE * TILE
+
+            @pl.loop(0, whole // TILE)
+            def _(tile):
+                step(pl.multiple_of(tile * TILE, TILE), TILE)
+
+            if last - first > whole:
+                step(whole, last - first - whole)
+            span = pl.ds(0 if c == 0 else gate_at, 2 * padded + (256 if c == 0 else 0))
+            going.append(
+                exchange(
+                    stage + c,
+                    "kv",
+                    lambda peer: send.at[peer, :, span],
+                    recv,
+                    lambda target: target.at[kv, :, span],
+                )
+            )
+        spreading = []
+        factor = None
+        for c, (first, last) in enumerate(chunks):
+            arrive(going[c])
+            if factor is None:
+                factor = row_factor(send, recv, 0)
+            width = last - first
+            gate_at = 256 + 2 * first
+            gate = factor * gathered_sum(send, recv, pl.ds(gate_at, width))
+            up = factor * gathered_sum(send, recv, pl.ds(gate_at + ceil_lanes(width), width))
+            hidden_all[which, kv, :, first:last] = (silu(gate) * up).astype(jnp.bfloat16)
+            span = pl.ds(first, ceil_lanes(width))
+            spreading.append(
+                exchange(
+                    stage + count + c,
+                    "kv",
+                    lambda peer: hidden_all.at[which, kv, :, span],
+                    hidden_all.at[which],
+                    lambda target: target.at[kv, :, span],
+                )
+            )
+        down_wait.wait()
+        for c, (first, last) in enumerate(chunks):
+            arrive(spreading[c])
+            hidden = (
+                hidden_all[which, :, :, first:last]
+                .astype(jnp.float32)
+                .reshape(rows, last - first)
+                .astype(jnp.bfloat16)
+            )
+            weight = down_v.at[which, pl.ds(first, last - first)]
+            if c < count - 1:
+                for t in range(n_tp):
+                    product = jnp.dot(
+                        hidden, weight[:, t * fb : (t + 1) * fb], preferred_element_type=jnp.float32
+                    )
+                    down_acc[t] = product if c == 0 else down_acc[t] + product
+        return down_exchange(
+            stage + 2 * count,
+            2 * which,
+            hidden,
+            weight,
+            0.5,
+            residual,
+            down_acc if count > 1 else None,
+        )
+
+    def spread(stage, which):
+        arrive(
+            exchange(stage, "tp", lambda peer: feat_all.at[which, tp], feat_all.at[which])
+        )
+
+    gains_all[tp] = jnp.concatenate(
+        [g[...].astype(jnp.float32) for g in (gain_in, gain_mix, gain_out)]
+        + [jnp.zeros((5, fb), jnp.float32)],
+        axis=0,
+    )
+    feat_all[0, tp] = tokens[...]
+    pl.semaphore_wait(barrier, n_kv + n_tp - 2)
+    feature_copies = exchange(0, "tp", lambda peer: feat_all.at[0, tp], feat_all.at[0])
+    gain_copies = exchange(1, "tp", lambda peer: gains_all.at[tp], gains_all)
+    lane = lax.broadcasted_iota(jnp.int32, (own, dk), 1)
+    line = lax.broadcasted_iota(jnp.int32, (own, dk), 0)
+    place = jnp.zeros((own, dk), jnp.float32)
+    for r in range(own):
+        place = jnp.where(line == r, positions[r].astype(jnp.float32), place)
+    half = jnp.where(lane < dk // 2, lane, lane - dk // 2).astype(jnp.float32)
+    cosine, sine = sine_pair(place * jnp.exp(half * (-2.0 * math.log(10000.0) / dk)))
+    sine = jnp.where(lane < dk // 2, -sine, sine)
+    arrive(feature_copies)
+    arrive(gain_copies)
+
+    after_first = half_block(
+        0, 10, 0, [first_loads[2 * c : 2 * c + 2] for c in range(len(chunks))], loads[0], tokens[...]
+    )
+    feat_all[1, tp] = after_first
+    spread(2, 1)
+
+    feats, normed = block(1, 1)
+    widths = (heads * dk, heads * dk, heads * dv, heads * dv)
+    total_width = sum(widths)
+    put_squares(proj_send, total_width, feats)
+    start = 0
+    for weight, load, width in zip((query_v, key_v, value_v, gates_v), loads[1:5], widths):
+        load.wait()
+        for column in range(0, width, TILE):
+            size = min(TILE, width - column)
+            put_rows(
+                proj_send,
+                pl.ds(start + column, size),
+                jnp.dot(
+                    normed, weight[:, column : column + size], preferred_element_type=jnp.float32
+                ),
+            )
+        start += width
+    arrive(exchange(3, "kv", lambda peer: proj_send.at[peer], proj_recv))
+    factor = row_factor(proj_send, proj_recv, total_width)
+    projected = (factor * gathered_sum(proj_send, proj_recv, pl.ds(0, total_width))).astype(
+        jnp.bfloat16
+    ).astype(jnp.float32)
+    loads[5].wait()
+    kept = []
+    for h in range(heads):
+        query = projected[:, h * dk : (h + 1) * dk]
+        key = projected[:, (heads + h) * dk : (heads + h + 1) * dk]
+        at = 2 * heads * dk + h * dv
+        value = projected[:, at : at + dv]
+        gate = projected[:, at + heads * dv : at + (heads + 1) * dv]
+        query = query * cosine + pltpu.roll(query, dk // 2, axis=1) * sine
+        key = (key * cosine + pltpu.roll(key, dk // 2, axis=1) * sine) * dk**-0.5
+        query_t, key_t = query.T, key.T
+        decay = jnp.exp(jnp.full((1, dv), -forget[h], jnp.float32))
+        carried = jnp.concatenate(
+            [
+                jnp.sum(query_t[:, b : b + 1] * state_v[b, h], axis=0, keepdims=True)
+                for b in range(own)
+            ],
+            axis=0,
+        )
+        retained = jnp.sum(query * key, axis=1, keepdims=True) * value + decay * carried
+        scaled = retained * lax.rsqrt(
+            jnp.sum(retained * retained, axis=1, keepdims=True) / dv + epsilon
+        )
+        mixed_all[kv, :, h * dv : (h + 1) * dv] = (silu(gate) * scaled).astype(jnp.bfloat16)
+        kept.append((key_t, value, decay))
+    mixed_copies = exchange(4, "kv", lambda peer: mixed_all.at[kv], mixed_all)
+    for h, (key_t, value, decay) in enumerate(kept):
+        for b in range(own):
+            state_v[b, h] = decay * state_v[b, h] + key_t[:, b : b + 1] * value[b : b + 1]
+    store = pltpu.make_async_copy(state_v, new_state, store_sem)
+    store.start()
+    arrive(mixed_copies)
+    loads[6].wait()
+    mixed = mixed_all[...].astype(jnp.float32).reshape(rows, heads * dv).astype(jnp.bfloat16)
+    second = down_exchange(5, 1, mixed, mixout_v, 1.0, after_first)
+    feat_all[2, tp] = second
+    spread(6, 2)
+
+    result[...] = half_block(
+        1,
+        11 + 2 * len(chunks),
+        2,
+        [loads[7:9]] + [[]] * (len(chunks) - 1),
+        loads[9],
+        second,
+    )
+    store.wait()
+    for copy in sent:
+        copy.wait_send()
+
+
+def fused_layer(
+    n_kv,
+    n_tp,
+    tokens,
+    gain_in,
+    gate_in,
+    up_in,
+    down_in,
+    gain_mix,
+    w_query,
+    w_key,
+    w_value,
+    w_gate,
+    w_mixout,
+    forget_rate,
+    state_in,
+    positions,
+    gain_out,
+    gate_out,
+    up_out,
+    down_out,
+):
+    rows, fb = tokens.shape
+    blk, ff = gate_in.shape
+    own, heads, dk, dv = state_in.shape
+    ffp = ceil_lanes(ff)
+    bf16 = jnp.bfloat16
+    proj_width = 2 * heads * (dk + dv) + 256
+    n_most = max(n_kv, n_tp)
+    vmem = pl.BlockSpec(memory_space=pltpu.VMEM)
+    smem = pl.BlockSpec(memory_space=pltpu.SMEM)
+    hbm = pl.BlockSpec(memory_space=pl.ANY)
+    gate_in, up_in, gate_out, up_out = gate_in.T, up_in.T, gate_out.T, up_out.T
+    stages = 12 + 4 * len(chunk_bounds(ff))
+    weights = (gate_in, up_in, down_in, w_query, w_key, w_value, w_gate, w_mixout)
+    weights += (state_in, gate_out, up_out, down_out)
+    return pl.pallas_call(
+        functools.partial(layer_kernel, n_kv, n_tp),
+        out_shape=(
+            jax.ShapeDtypeStruct(tokens.shape, bf16),
+            jax.ShapeDtypeStruct(state_in.shape, jnp.float32),
+        ),
+        in_specs=[vmem] * 4 + [smem] * 2 + [hbm] * len(weights),
+        out_specs=(vmem, hbm),
+        scratch_shapes=[
+            pltpu.VMEM((2, ff, blk), bf16),
+            pltpu.VMEM((2, ff, blk), bf16),
+            pltpu.VMEM((2,) + down_in.shape, bf16),
+            pltpu.VMEM(w_query.shape, bf16),
+            pltpu.VMEM(w_key.shape, bf16),
+            pltpu.VMEM(w_value.shape, bf16),
+            pltpu.VMEM(w_gate.shape, bf16),
+            pltpu.VMEM(w_mixout.shape, bf16),
+            pltpu.VMEM(state_in.shape, jnp.float32),
+            pltpu.VMEM((n_tp, 8, fb), jnp.float32),
+            pltpu.VMEM((3, n_tp, rows, fb), bf16),
+            pltpu.VMEM((2, n_kv, own, 2 * ffp + 256), bf16),
+            pltpu.VMEM((2, n_kv, own, 2 * ffp + 256), bf16),
+            pltpu.VMEM((2, n_kv, own, ffp), bf16),
+            pltpu.VMEM((n_tp, rows, fb), jnp.float32),
+            pltpu.VMEM((n_kv, own, proj_width), bf16),
+            pltpu.VMEM((n_kv, own, proj_width), bf16),
+            pltpu.VMEM((n_kv, own, heads * dv), bf16),
+            pltpu.VMEM((3, n_tp, rows, fb), bf16),
+            pltpu.VMEM((3, n_tp, rows, fb), bf16),
+            pltpu.SemaphoreType.DMA((10 + 2 * len(chunk_bounds(ff)),)),
+            pltpu.SemaphoreType.DMA,
+            pltpu.SemaphoreType.DMA((stages, n_most)),
+            pltpu.SemaphoreType.DMA((stages, n_most)),
+        ],
+        compiler_params=pltpu.CompilerParams(
+            collective_id=0, has_side_effects=True, vmem_limit_bytes=60 * 2**20
+        ),
+        name="fused_layer",
+    )(
+        tokens,
+        gain_in[None, :],
+        gain_mix[None, :],
+        gain_out[None, :],
+        forget_rate,
+        positions,
+        *weights,
+    )
+
+
+def choose(n_kv, n_tp, *arguments):
+    tokens, gate_in, state_in = arguments[0], arguments[2], arguments[12]
+    aligned = (
+        tokens.shape[1] % 128 == 0
+        and gate_in.shape[0] % 128 == 0
+        and state_in.shape[0] == 8
+        and state_in.shape[2] == 128
+    )
+    if aligned:
+        return fused_layer(n_kv, n_tp, *arguments)
+    return on_device(*arguments)
+
+
 def solution(mesh):
     in_specs = (
         P("grp", ("kv", "tp")),
@@ -153,6 +663,7 @@
         P("tp", "kv"),
     )
     out_specs = (P("grp", ("kv", "tp")), P(("grp", "kv"), "tp", None, None))
+    body = functools.partial(choose, mesh.shape["kv"], mesh.shape["tp"])
     return jax.shard_map(
-        on_device, mesh=mesh, in_specs=in_specs, out_specs=out_specs, check_vma=False
-    )
+        body, mesh=mesh, in_specs=in_specs, out_specs=out_specs, check_vma=False
+    )

time: 263 us -> 70.7 us (0.27)
  waiting for transfers between devices: 112 us -> 0 us
  blocking collectives: 93.6 us -> 0 us
  Pallas kernels: 0 us -> 61.6 us
  matrix products: 34.2 us -> 0 us
  between operations: 14.3 us -> 0.64 us
  local copies, waits for them, and re-layouts: 0.96 us -> 8.11 us
  other arithmetic: 6.92 us -> 0 us
    all_gather x7 -> x0, blocking collectives: 76.2 us -> none  [the longest x3 39.6 us: block_rows(): lax.all_gather(tokens, 'tp', axis=1, tiled=True)]
    reduce_scatter x4 -> x0, waiting for transfers between devices: 63.6 us -> none  [the longest x2 37.2 us: half_mlp(): lax.psum_scatter(partial_value.astype(jnp.bfloat16), 'tp', scatter_dimens...]
    pallas_call x0 -> x1, Pallas kernels: none -> 61.6 us  [fused_layer(): pl.pallas_call(functools.partial(layer_kernel, n_kv, n_tp), out_shape=(ja...]
    psum x2 -> x0, waiting for transfers between devices: 48.2 us -> none  [half_mlp(): lax.psum(up_part.astype(jnp.bfloat16), 'kv').astype(jnp.float32)]
    dot_general x12 -> x0, matrix products: 34.2 us -> none  [the longest x2 10.1 us: half_mlp(): up_part = jnp.dot(normed, w_up, preferred_element_type=jnp.float32)]
    psum x3 -> x0, blocking collectives: 17.4 us -> none  [block_rows(): squares = lax.psum(jnp.sum(wide_block * wide_block, axis=1), 'kv')]
    broadcast_in_dim x0 -> x3, local copies, waits for them, and re-layouts: none -> 3.69 us  [the longest x1 1.25 us: fused_layer(): gain_out[None, :]]
    convert_element_type x7 -> x0, other arithmetic: 3.68 us -> none  [the longest x2 2.06 us: half_mlp(): return (widened + 0.5 * lowered).astype(jnp.bfloat16)]
  transfers between devices with their start and end apart: 6 -> 0, of which waited for: 6 -> 0; matrix products, arithmetic and copies ran while one was open for 1% -> 0% of each run, Pallas kernels for 0% -> 0%
where the time goes in v1:
time: 70.7 us; the launch traced here: 70.4 us
  Pallas kernels  61.6 us (87%)
  local copies, waits for them, and re-layouts  8.11 us (11%)
    pallas_call x1, Pallas kernels, fused_layer(): pl.pallas_call(functools.partial(layer_kernel, n_kv, n_tp), out_shape=(ja...  61.6 us
    unnamed x2, local copies, waits for them, and re-layouts  4.42 us

profile of v1, /device:TPU:0, one launch (start us, length us, event | category | flops | bytes accessed | tf_op | source)
XLA Modules:
  0.0 70.4 jit_solution(6443189603321672080)
XLA Ops:
  0.6 1.2 %broadcast_in_dim.9.gain_in = bf16[1,256]{1,0:T(2,128)(2,1)} reshape(bf16[256]{0:T(256)(128)(2,1)} %param.19) | data formatting | bytes 1024 | tf_op jit(solution)/shard_map/broadcast_in_dim | solution.py:622
  1.8 1.2 %broadcast_in_dim.10.gain_mix = bf16[1,256]{1,0:T(2,128)(2,1)} reshape(bf16[256]{0:T(256)(128)(2,1)} %param.23) | data formatting | bytes 1024 | tf_op jit(solution)/shard_map/broadcast_in_dim | solution.py:623
  3.1 1.2 %broadcast_in_dim.11.gain_out = bf16[1,256]{1,0:T(2,128)(2,1)} reshape(bf16[256]{0:T(256)(128)(2,1)} %param.32) | data formatting | bytes 1024 | tf_op jit(solution)/shard_map/broadcast_in_dim | solution.py:624
  4.3 61.6 %fused_layer.1 = (bf16[32,256]{1,0:T(8,128)(2,1)}, f32[8,2,128,256]{3,2,1,0:T(8,128)}) custom-call(bf16[32,256]{1,0:T(8,128)(2,1)} %tokens.1, bf16[1,256]{1,0:T(2,128)(2,1)} %broadcast_in_dim.9.gain_in, bf16[1,256]{1,0:T(2,128)(2,1)} %broadcast_in_dim.10.gain_mix, bf16[1,256]{1,0:T(2,128)(2,1)} %broadcast_in_dim.11.gain_out, f32[2]{0:T(128)} %forget.1, ...), custom_call_target="tpu_custom_call" | custom-call | tf_op jit(solution)/shard_map/fused_layer/pallas_call | solution.py:582
  66.0 1.3 %copy.22 = bf16[32,256]{1,0:T(8,128)(2,1)} copy(bf16[32,256]{1,0:T(8,128)(2,1)} %get-tuple-element.4) | data formatting | bytes 32768
  67.3 3.1 %copy.23 = f32[8,2,128,256]{3,2,1,0:T(8,128)} copy(f32[8,2,128,256]{3,2,1,0:T(8,128)} %get-tuple-element.5) | data formatting | bytes 4194304

commit v2 on v1

--- a/solution.py
+++ b/solution.py
@@ -138,7 +138,7 @@
 
 MESH = pl.DeviceIdType.MESH
 TILE = 256
-CHUNKS = 3
+CHUNKS = 5
 
 
 def chunk_bounds(width):

time: 70.7 us -> 70.4 us (level)
  no operation moved by 1% of the time
where the time goes in v2:
time: 70.4 us; the launch traced here: 70.1 us
  Pallas kernels  61.4 us (87%)
  local copies, waits for them, and re-layouts  8.11 us (12%)
    pallas_call x1, Pallas kernels, fused_layer(): pl.pallas_call(functools.partial(layer_kernel, n_kv, n_tp), out_shape=(ja...  61.4 us
    unnamed x2, local copies, waits for them, and re-layouts  4.42 us

profile of v2, /device:TPU:0, one launch (start us, length us, event | category | flops | bytes accessed | tf_op | source)
XLA Modules:
  0.0 70.1 jit_solution(6721907143772670638)
XLA Ops:
  0.6 1.2 %broadcast_in_dim.9.gain_in = bf16[1,256]{1,0:T(2,128)(2,1)} reshape(bf16[256]{0:T(256)(128)(2,1)} %param.19) | data formatting | bytes 1024 | tf_op jit(solution)/shard_map/broadcast_in_dim | solution.py:622
  1.8 1.2 %broadcast_in_dim.10.gain_mix = bf16[1,256]{1,0:T(2,128)(2,1)} reshape(bf16[256]{0:T(256)(128)(2,1)} %param.23) | data formatting | bytes 1024 | tf_op jit(solution)/shard_map/broadcast_in_dim | solution.py:623
  3.1 1.2 %broadcast_in_dim.11.gain_out = bf16[1,256]{1,0:T(2,128)(2,1)} reshape(bf16[256]{0:T(256)(128)(2,1)} %param.32) | data formatting | bytes 1024 | tf_op jit(solution)/shard_map/broadcast_in_dim | solution.py:624
  4.3 61.4 %fused_layer.1 = (bf16[32,256]{1,0:T(8,128)(2,1)}, f32[8,2,128,256]{3,2,1,0:T(8,128)}) custom-call(bf16[32,256]{1,0:T(8,128)(2,1)} %tokens.1, bf16[1,256]{1,0:T(2,128)(2,1)} %broadcast_in_dim.9.gain_in, bf16[1,256]{1,0:T(2,128)(2,1)} %broadcast_in_dim.10.gain_mix, bf16[1,256]{1,0:T(2,128)(2,1)} %broadcast_in_dim.11.gain_out, f32[2]{0:T(128)} %forget.1, ...), custom_call_target="tpu_custom_call" | custom-call | tf_op jit(solution)/shard_map/fused_layer/pallas_call | solution.py:582
  65.7 1.3 %copy.22 = bf16[32,256]{1,0:T(8,128)(2,1)} copy(bf16[32,256]{1,0:T(8,128)(2,1)} %get-tuple-element.4) | data formatting | bytes 32768
  67.0 3.1 %copy.23 = f32[8,2,128,256]{3,2,1,0:T(8,128)} copy(f32[8,2,128,256]{3,2,1,0:T(8,128)} %get-tuple-element.5) | data formatting | bytes 4194304
